TPU v7x, 128 devices: a whole 4x4x4 slice. The times are simulated.
128 devices in a mesh: fs: 16 (over z, y), tp: 8 (over x, core).
Axes of the slice: x: 4, y: 4, z: 4, core: 2. Of those that a mesh axis runs over, the one named last changes fastest.
Arguments:
- tokens: bfloat16 [16384, 2048], P('fs', 'tp'), may hold values from -40 to 40
- first_gain: float32 [2048], replicated, may hold values from 0.1 to 1.9
- first_gate: bfloat16 [2048, 6144], P('fs', 'tp'), may hold values from -0.125 to 0.125
- first_upward: bfloat16 [2048, 6144], P('fs', 'tp'), may hold values from -0.125 to 0.125
- first_down: bfloat16 [6144, 2048], P('tp', 'fs'), may hold values from -0.078125 to 0.078125
- mix_gain: float32 [2048], replicated, may hold values from 0.1 to 1.9
- mix_input: bfloat16 [2048, 1024], P('fs', 'tp'), may hold values from -0.125 to 0.125
- pool_weight: bfloat16 [8, 128, 128], replicated, may hold values from -0.5 to 0.5
- pool_scale: float32 [1024], replicated, may hold values from 0.1 to 1.9
- mix_output: bfloat16 [1024, 2048], P('tp', 'fs'), may hold values from -0.1875 to 0.1875
- second_gain: float32 [2048], replicated, may hold values from 0.1 to 1.9
- second_gate: bfloat16 [2048, 6144], P('fs', 'tp'), may hold values from -0.125 to 0.125
- second_upward: bfloat16 [2048, 6144], P('fs', 'tp'), may hold values from -0.125 to 0.125
- second_down: bfloat16 [6144, 2048], P('tp', 'fs'), may hold values from -0.078125 to 0.078125
Outputs:
- layer_out: bfloat16 [16384, 2048], P('fs', 'tp')
All inputs are finite; a program needn't handle non-finite values.
Results may differ from a plain program's by a relative error of at most 0.01.
Values may be sent and summed in bfloat16 or wider, within the bound.
A program may use at most 128 MiB of HBM per device.

v0:
```python
import jax
import jax.numpy as jnp
from jax import lax
from jax.sharding import Mesh
from jax.sharding import PartitionSpec as P

GROUP_DIM = 128
FS = ("fs_0", "fs_1")


EPSILON = 1e-06
REACH = 15


def in_one_piece(arrays, axis, dim, along):
    widths = [a.shape[along] for a in arrays]
    both = jnp.concatenate(arrays, axis=along)
    out = lax.all_gather(both, axis, axis=dim, tiled=True)
    return tuple(jnp.split(out, [sum(widths[:k]) for k in range(1, len(widths))], axis=along))


def gathered_by_axis(array, axes, dim):
    out = array
    for number in range(len(axes) - 1, -1, -1):
        out = lax.all_gather(out, axes[number], axis=dim, tiled=True)
    return out


def shifted_2(value, axis, steps):
    count = lax.axis_size(axis)
    initial, last = (max(0, -steps), min(count, count - steps))
    return lax.ppermute(value, axis, [(source, source + steps) for source in range(initial, last)])


def normalize(values, weight_gain):
    wide = values.astype(jnp.float32)
    factor = lax.rsqrt(jnp.mean(wide * wide, axis=-1, keepdims=True) + EPSILON)
    return (wide * factor * weight_gain).astype(jnp.bfloat16)


def gather_rows(shard):
    return lax.all_gather(shard, "tp", axis=1, tiled=True)


def feed_forward(shard, weight_gain, gate_weight, upward_weight, down_weight):
    normed = normalize(gather_rows(shard), weight_gain)
    pieces = in_one_piece((gate_weight, upward_weight), FS, 0, 1)
    gated = jnp.dot(normed, pieces[0], preferred_element_type=jnp.float32)
    upward = jnp.dot(normed, pieces[1], preferred_element_type=jnp.float32)
    hidden = (jax.nn.silu(gated) * upward).astype(jnp.bfloat16)
    partial_value = jnp.dot(
        hidden, gathered_by_axis(down_weight, FS, 1), preferred_element_type=jnp.float32
    )
    partial_value = partial_value.astype(jnp.bfloat16).astype(jnp.float32)
    summed = lax.psum_scatter(
        partial_value.astype(jnp.bfloat16), "tp", scatter_dimension=1, tiled=True
    ).astype(jnp.float32)
    return (shard.astype(jnp.float32) + 0.5 * summed).astype(jnp.bfloat16)


def pool_groups(extended, positions, pool_weight, pool_scale):
    row_count = positions.shape[0]
    group_count = extended.shape[1] // GROUP_DIM
    group_ids = jnp.arange(group_count, dtype=jnp.int32)
    windows = jnp.left_shift(2, group_ids % 4)
    window_cols = jnp.repeat(windows, GROUP_DIM)[None, :]
    wide = extended.astype(jnp.float32)
    summed = jnp.zeros((row_count, wide.shape[1]), jnp.float32)
    for offset in range(REACH + 1):
        shifted = wide[REACH - offset : REACH - offset + row_count]
        summed = summed + jnp.where(offset < window_cols, shifted, 0.0)
    counts = jnp.minimum(positions[:, None] + 1, window_cols).astype(jnp.float32)
    pooled = (summed / counts - wide[REACH:]).astype(jnp.bfloat16)
    mapped = jnp.einsum(
        "tgc,gcd->tgd",
        pooled.reshape(row_count, group_count, GROUP_DIM),
        pool_weight,
        preferred_element_type=jnp.float32,
    )
    return (mapped.reshape(row_count, group_count * GROUP_DIM) * pool_scale).astype(jnp.bfloat16)


def per_device(
    tokens,
    first_gain,
    first_gate,
    first_upward,
    first_down,
    mix_gain,
    mix_input,
    pool_weight,
    pool_scale,
    mix_output,
    second_gain,
    second_gate,
    second_upward,
    second_down,
):
    first_out = feed_forward(tokens, first_gain, first_gate, first_upward, first_down)
    input_rows, output_cols = (
        lax.all_gather(mix_input, FS, axis=0, tiled=True),
        lax.all_gather(mix_output, FS, axis=1, tiled=True),
    )
    full_input, full_output = (
        lax.all_gather(input_rows, "tp", axis=1, tiled=True),
        lax.all_gather(output_cols, "tp", axis=0, tiled=True),
    )
    run_rows = lax.all_to_all(first_out, "tp", split_axis=0, concat_axis=1, tiled=True)
    normed = normalize(run_rows, mix_gain)
    pool_in = jnp.dot(normed, full_input, preferred_element_type=jnp.float32).astype(jnp.bfloat16)
    row_count = pool_in.shape[0]
    prior = shifted_2(pool_in[row_count - REACH :], "tp", 1)
    extended = jnp.concatenate([prior, pool_in], 0)
    positions = lax.axis_index("tp") * row_count + jnp.arange(row_count, dtype=jnp.int32)
    mapped = pool_groups(extended, positions, pool_weight, pool_scale)
    blocks = lax.axis_size("tp")
    width = mapped.shape[1] // blocks
    result = jnp.zeros((row_count, full_output.shape[1]), jnp.float32)
    for block in range(blocks):
        piece = jnp.dot(
            mapped[:, block * width : (block + 1) * width],
            full_output[block * width : (block + 1) * width],
            preferred_element_type=jnp.float32,
        )
        result = result + piece.astype(jnp.bfloat16).astype(jnp.float32)
    mixer = lax.all_to_all(
        result.astype(jnp.bfloat16), "tp", split_axis=1, concat_axis=0, tiled=True
    ).astype(result.dtype)
    mid_out = (first_out.astype(jnp.float32) + mixer).astype(jnp.bfloat16)
    return feed_forward(mid_out, second_gain, second_gate, second_upward, second_down)


def solution(mesh):
    split = Mesh(mesh.devices.reshape(4, 4, mesh.shape["tp"]), ("fs_0", "fs_1", "tp"))
    return jax.shard_map(
        per_device,
        mesh=split,
        in_specs=(
            P(FS, "tp"),
            P(),
            P(FS, "tp"),
            P(FS, "tp"),
            P("tp", FS),
            P(),
            P(FS, "tp"),
            P(),
            P(),
            P("tp", FS),
            P(),
            P(FS, "tp"),
            P(FS, "tp"),
            P("tp", FS),
        ),
        out_specs=P(FS, "tp"),
        check_vma=False,
    )
```

profile of v0, /device:TPU:1, one launch (start us, length us, event | category | flops | bytes accessed | tf_op | source)
XLA Modules:
  0.0 497.5 jit_solution(2457293997818745724)
XLA Ops:
  7.3 1.8 pad_maximum_fusion
  9.2 19.2 %all_gather.38 = bf16[768,512]{1,0:T(8,128)(2,1)} all-gather(bf16[768,128]{1,0:T(8,128)(2,1)} %param.18), channel_id=1, replica_groups=mesh['fs_0'=4,'fs_1'=4,'tp'=8] {'fs_1'}, dimensions={1}, use_global_device_ids=true | all-gather | bytes 983040 | tf_op jit(solution)/shard_map/all_gather | solution.py:25
  28.5 19.7 %all-gather.9.cloned.1.call-done = bf16[1024,2048]{1,0:T(8,128)(2,1)} async-done(((bf16[1024,256]{1,0:T(8,128)(2,1)}), bf16[1024,2048]{1,0:T(8,128)(2,1)}) %all-gather.9.cloned.1.call-update) | async-done | bytes 4194320 | tf_op jit(solution)/shard_map/all_gather | solution.py:42
  48.1 3.1 fusion
  51.2 60.9 %all-gather.11.cloned.1.call-done = bf16[2048,1536]{1,0:T(8,128)(2,1)} async-done(((bf16[128,1536]{1,0:T(8,128)(2,1)}), bf16[2048,1536]{1,0:T(8,128)(2,1)}) %all-gather.11.cloned.1.call-update) | async-done | bytes 6291472 | tf_op jit(solution)/shard_map/all_gather | solution.py:18
  112.1 6.4 %fusion.10 = f32[1024,768]{1,0:T(8,128)S(1)} fusion(bf16[2048,1536]{1,0:T(8,128)(2,1)} %all-gather.11.cloned.1.call-done, bf16[1024,2048]{1,0:T(8,128)(2,1)} %all-gather.9.cloned.1.call-done, f32[2048]{0:T(1024)S(1)} %copy-done.12, f32[1024]{0:T(1024)S(1)} %add_rsqrt_fusion.1), kind=kOutput, calls=%fused_computation.16 | convolution fusion | flops 3229614080 | bytes 10498048 | tf_op jit(solution)/shard_map/dot_general | solution.py:49
  118.5 34.5 %all-gather.13.cloned.1.call-done = bf16[768,2048]{1,0:T(8,128)(2,1)} async-done(((bf16[768,512]{1,0:T(8,128)(2,1)}), bf16[768,2048]{1,0:T(8,128)(2,1)}) %all-gather.13.cloned.1.call-update) | async-done | bytes 3145744 | tf_op jit(solution)/shard_map/all_gather | solution.py:25
  153.1 13.1 %convolution_convert_fusion.1 = bf16[1024,2048]{1,0:T(8,128)(2,1)} fusion(bf16[768,2048]{1,0:T(8,128)(2,1)} %all-gather.13.cloned.1.call-done, f32[1024,768]{1,0:T(8,128)S(1)} %fusion.10, bf16[2048,1536]{1,0:T(8,128)(2,1)} %all-gather.11.cloned.1.call-done, bf16[1024,2048]{1,0:T(8,128)(2,1)} %all-gather.9.cloned.1.call-done, f32[2048]{0:T(1024)S(1)} %copy-done.12, ...), kind=kOutput, calls=%fused_computation.11 | convolution fusion | flops 6457655296 | bytes 17838080 | tf_op jit(solution)/shard_map/dot_general | solution.py:51
  166.9 21.0 %all_gather.40 = bf16[2048,128]{1,0:T(8,128)(2,1)} all-gather(bf16[128,128]{1,0:T(8,128)(2,1)S(1)} %copy-done.8), channel_id=1, replica_groups=mesh['fs_0'=4,'fs_1'=4,'tp'=8] {'fs_0','fs_1'}, dimensions={0}, use_global_device_ids=true | all-gather | bytes 557056 | tf_op jit(solution)/shard_map/all_gather | solution.py:101
  188.0 20.2 %all_gather.42 = bf16[128,2048]{1,0:T(8,128)(2,1)} all-gather(bf16[128,128]{1,0:T(8,128)(2,1)S(1)} %copy-done.9), channel_id=1, replica_groups=mesh['fs_0'=4,'fs_1'=4,'tp'=8] {'fs_0','fs_1'}, dimensions={1}, use_global_device_ids=true | all-gather | bytes 557056 | tf_op jit(solution)/shard_map/all_gather | solution.py:102
  208.2 1.2 add_convert_fusion.1
  209.5 1.0 copy.18
  210.5 13.9 %all-to-all-start = ((bf16[8,128,256]{1,2,0:T(8,128)(2,1)}), bf16[8,128,256]{1,2,0:T(8,128)(2,1)S(1)}, u32[]{:S(2)}, u32[]{:S(2)}) async-start(bf16[8,128,256]{1,2,0:T(8,128)(2,1)} %copy.18), calls=%async_computation.1 | async-start | bytes 1048576 | tf_op jit(solution)/shard_map/all_to_all | solution.py:108
  224.5 14.2 %all-to-all-done = bf16[8,128,256]{1,2,0:T(8,128)(2,1)S(1)} async-done(((bf16[8,128,256]{1,2,0:T(8,128)(2,1)}), bf16[8,128,256]{1,2,0:T(8,128)(2,1)S(1)}, u32[]{:S(2)}, u32[]{:S(2)}) %all-to-all-start) | async-done | bytes 524320 | tf_op jit(solution)/shard_map/all_to_all | solution.py:108
  239.3 8.0 %all-gather.15.cloned.1.call-done = bf16[2048,1024]{1,0:T(8,128)(2,1)} async-done(((bf16[2048,128]{1,0:T(8,128)(2,1)}), bf16[2048,1024]{1,0:T(8,128)(2,1)}) %all-gather.15.cloned.1.call-update) | async-done | bytes 4194320 | tf_op jit(solution)/shard_map/all_gather | solution.py:105
  247.3 2.9 convolution_convert_fusion.10
  250.2 2.1 collective-permute-start
  252.3 1.0 collective-permute-done
  253.4 1.5 fusion.76
  255.2 26.0 %all-gather.17.cloned.1.call-done = bf16[1024,2048]{1,0:T(8,128)(2,1)} async-done(((bf16[128,2048]{1,0:T(8,128)(2,1)}), bf16[1024,2048]{1,0:T(8,128)(2,1)}) %all-gather.17.cloned.1.call-update) | async-done | bytes 4194320 | tf_op jit(solution)/shard_map/all_gather | solution.py:106
  281.1 1.5 fusion.29
  282.6 1.4 fusion.28
  286.1 12.3 %all_to_all.26 = bf16[128,8,256]{2,0,1:T(8,128)(2,1)S(1)} all-to-all(bf16[128,8,256]{2,0,1:T(8,128)(2,1)S(1)} %bitcast.56), channel_id=1, replica_groups=mesh['fs_0'=4,'fs_1'=4,'tp'=8] {'tp'}, dimensions={1} | all-to-all | bytes 1048576 | tf_op jit(solution)/shard_map/all_to_all | solution.py:126
  300.3 16.2 %all_gather.46 = bf16[768,512]{1,0:T(8,128)(2,1)} all-gather(bf16[768,128]{1,0:T(8,128)(2,1)S(1)} %copy-done.7), channel_id=1, replica_groups=mesh['fs_0'=4,'fs_1'=4,'tp'=8] {'fs_1'}, dimensions={1}, use_global_device_ids=true | all-gather | bytes 983040 | tf_op jit(solution)/shard_map/all_gather | solution.py:25
  316.5 18.7 %all-gather.19.cloned.1.call-done = bf16[1024,2048]{1,0:T(8,128)(2,1)} async-done(((bf16[1024,256]{1,0:T(8,128)(2,1)}), bf16[1024,2048]{1,0:T(8,128)(2,1)}) %all-gather.19.cloned.1.call-update) | async-done | bytes 4194320 | tf_op jit(solution)/shard_map/all_gather | solution.py:42
  335.2 3.1 fusion.3
  338.3 60.9 %all-gather.21.cloned.1.call-done = bf16[2048,1536]{1,0:T(8,128)(2,1)} async-done(((bf16[128,1536]{1,0:T(8,128)(2,1)}), bf16[2048,1536]{1,0:T(8,128)(2,1)}) %all-gather.21.cloned.1.call-update) | async-done | bytes 6291472 | tf_op jit(solution)/shard_map/all_gather | solution.py:18
  399.1 6.4 %fusion.6 = f32[1024,768]{1,0:T(8,128)S(1)} fusion(bf16[2048,1536]{1,0:T(8,128)(2,1)} %all-gather.21.cloned.1.call-done, bf16[1024,2048]{1,0:T(8,128)(2,1)} %all-gather.19.cloned.1.call-done, f32[2048]{0:T(1024)S(1)} %copy-done.13, f32[1024]{0:T(1024)S(1)} %add_rsqrt_fusion), kind=kOutput, calls=%fused_computation.12 | convolution fusion | flops 3229614080 | bytes 10498048 | tf_op jit(solution)/shard_map/dot_general | solution.py:49
  405.6 34.6 %all-gather.23.cloned.1.call-done = bf16[768,2048]{1,0:T(8,128)(2,1)} async-done(((bf16[768,512]{1,0:T(8,128)(2,1)}), bf16[768,2048]{1,0:T(8,128)(2,1)}) %all-gather.23.cloned.1.call-update) | async-done | bytes 3145744 | tf_op jit(solution)/shard_map/all_gather | solution.py:25
  440.1 13.1 %convolution_convert_fusion = bf16[1024,2048]{1,0:T(8,128)(2,1)} fusion(bf16[768,2048]{1,0:T(8,128)(2,1)} %all-gather.23.cloned.1.call-done, f32[1024,768]{1,0:T(8,128)S(1)} %fusion.6, bf16[2048,1536]{1,0:T(8,128)(2,1)} %all-gather.21.cloned.1.call-done, bf16[1024,2048]{1,0:T(8,128)(2,1)} %all-gather.19.cloned.1.call-done, f32[2048]{0:T(1024)S(1)} %copy-done.13, ...), kind=kOutput, calls=%fused_computation.10 | convolution fusion | flops 6457655296 | bytes 17838080 | tf_op jit(solution)/shard_map/dot_general | solution.py:51
  453.2 35.4 %reduce-scatter.5.cloned.1.call-done = bf16[1024,256]{1,0:T(8,128)(2,1)} async-done(((bf16[1024,2048]{1,0:T(8,128)(2,1)}), bf16[1024,256]{1,0:T(8,128)(2,1)}) %reduce-scatter.5.cloned.1.call-update) | async-done | bytes 524304 | tf_op jit(solution)/shard_map/reduce_scatter | solution.py:55
  488.7 2.0 add_convert_fusion
  (70 shorter events, 6.7 us)
Async XLA Ops:
  6.5 246.9 %copy-start = (bf16[8,128,128]{2,1,0:T(8,128)(2,1)S(1)}, bf16[8,128,128]{2,1,0:T(8,128)(2,1)}, u32[]{:S(2)}) copy-start(bf16[8,128,128]{2,1,0:T(8,128)(2,1)} %param.21) | copy-start | bytes 786436
  6.5 105.5 %copy-start.12 = (f32[2048]{0:T(1024)S(1)}, f32[2048]{0:T(1024)}, u32[]{:S(2)}) copy-start(f32[2048]{0:T(1024)} %param.15) | copy-start | bytes 24580
  6.5 41.6 %all-gather.9.cloned.1.call-start = ((), (), s32[]{:S(2)}) async-start(), calls=%async_computation.4 | async-start | bytes 4718592 | tf_op jit(solution)/shard_map/all_gather | solution.py:42
  7.3 104.8 %all-gather.11.cloned.1.call-start = ((), (), s32[]{:S(2)}) async-start(), calls=%async_computation.5 | async-start | bytes 6684672 | tf_op jit(solution)/shard_map/all_gather | solution.py:18
  9.1 143.9 %all-gather.13.cloned.1.call-start = ((), (), s32[]{:S(2)}) async-start(), calls=%async_computation.6 | async-start | bytes 3932160 | tf_op jit(solution)/shard_map/all_gather | solution.py:25
  28.4 179.8 %reduce-scatter.3.cloned.1.call-start = ((), (), s32[]{:S(2)}) async-start(), calls=%async_computation.7 | async-start | bytes 4718592 | tf_op jit(solution)/shard_map/reduce_scatter | solution.py:55
  166.2 0.8 copy-start.8
  166.2 21.9 %copy-start.9 = (bf16[128,128]{1,0:T(8,128)(2,1)S(1)}, bf16[128,128]{1,0:T(8,128)(2,1)}, u32[]{:S(2)}) copy-start(bf16[128,128]{1,0:T(8,128)(2,1)} %param.23) | copy-start | bytes 98308
  166.2 42.1 %copy-start.4 = (bf16[1024,256]{1,0:T(8,128)(2,1)S(1)}, bf16[1024,256]{1,0:T(8,128)(2,1)}, u32[]{:S(2)}) copy-start(bf16[1024,256]{1,0:T(8,128)(2,1)} %param.14) | copy-start | bytes 1572868
  166.2 72.8 %copy-start.10 = (f32[2048]{0:T(1024)S(1)}, f32[2048]{0:T(1024)}, u32[]{:S(2)}) copy-start(f32[2048]{0:T(1024)} %param.19) | copy-start | bytes 24580
  166.2 81.1 %all-gather.15.cloned.1.call-start = ((), (), s32[]{:S(2)}) async-start(), calls=%async_computation.8 | async-start | bytes 4718592 | tf_op jit(solution)/shard_map/all_gather | solution.py:105
  188.0 93.1 %all-gather.17.cloned.1.call-start = ((), (), s32[]{:S(2)}) async-start(), calls=%async_computation.9 | async-start | bytes 4718592 | tf_op jit(solution)/shard_map/all_gather | solution.py:106
  210.5 28.2 %all-to-all-start = ((bf16[8,128,256]{1,2,0:T(8,128)(2,1)}), bf16[8,128,256]{1,2,0:T(8,128)(2,1)S(1)}, u32[]{:S(2)}, u32[]{:S(2)}) async-start(bf16[8,128,256]{1,2,0:T(8,128)(2,1)} %copy.18), calls=%async_computation.1 | async-start | bytes 1048576 | tf_op jit(solution)/shard_map/all_to_all | solution.py:108
  224.3 110.9 %all-gather.19.cloned.1.call-start = ((), (), s32[]{:S(2)}) async-start(), calls=%async_computation.10 | async-start | bytes 4718592 | tf_op jit(solution)/shard_map/all_gather | solution.py:42
  250.2 3.1 collective-permute-start
  253.4 1.5 copy-start.11
  281.1 2.9 copy-start.3
  285.3 14.1 %copy-start.5 = (bf16[128,768]{1,0:T(8,128)(2,1)S(1)}, bf16[128,768]{1,0:T(8,128)(2,1)}, u32[]{:S(2)}) copy-start(bf16[128,768]{1,0:T(8,128)(2,1)} %param.26) | copy-start | bytes 589828
  285.4 14.1 %copy-start.6 = (bf16[128,768]{1,0:T(8,128)(2,1)S(1)}, bf16[128,768]{1,0:T(8,128)(2,1)}, u32[]{:S(2)}) copy-start(bf16[128,768]{1,0:T(8,128)(2,1)} %param.25) | copy-start | bytes 589828
  285.7 14.6 %copy-start.7 = (bf16[768,128]{1,0:T(8,128)(2,1)S(1)}, bf16[768,128]{1,0:T(8,128)(2,1)}, u32[]{:S(2)}) copy-start(bf16[768,128]{1,0:T(8,128)(2,1)} %param.27) | copy-start | bytes 589828
  299.3 99.8 %copy-start.13 = (f32[2048]{0:T(1024)S(1)}, f32[2048]{0:T(1024)}, u32[]{:S(2)}) copy-start(f32[2048]{0:T(1024)} %param.24) | copy-start | bytes 24580
  299.4 99.8 %all-gather.21.cloned.1.call-start = ((), (), s32[]{:S(2)}) async-start(), calls=%async_computation.11 | async-start | bytes 6684672 | tf_op jit(solution)/shard_map/all_gather | solution.py:18
  300.2 139.9 %all-gather.23.cloned.1.call-start = ((), (), s32[]{:S(2)}) async-start(), calls=%async_computation.12 | async-start | bytes 3932160 | tf_op jit(solution)/shard_map/all_gather | solution.py:25
  316.5 172.2 %reduce-scatter.5.cloned.1.call-start = ((), (), s32[]{:S(2)}) async-start(), calls=%async_computation.13 | async-start | bytes 4718592 | tf_op jit(solution)/shard_map/reduce_scatter | solution.py:55
  440.1 50.5 %copy-start.1 = (bf16[8,128,128]{2,1,0:T(8,128)(2,1)S(1)}, bf16[8,128,128]{2,1,0:T(8,128)(2,1)}, u32[]{:S(2)}) copy-start(bf16[8,128,128]{2,1,0:T(8,128)(2,1)} %param.21) | copy-start | bytes 786436
  453.2 35.4 %copy-start.2 = (bf16[1024,256]{1,0:T(8,128)(2,1)S(1)}, bf16[1024,256]{1,0:T(8,128)(2,1)}, u32[]{:S(2)}) copy-start(bf16[1024,256]{1,0:T(8,128)(2,1)} %fusion.46) | copy-start | bytes 1572868
Sparse Core Ops, SparseCore 0:
  9.0 39.0 all-gather.8
  50.3 61.7 all-gather.10
  113.7 39.2 all-gather.12
  166.3 35.4 reduce-scatter.2
  203.3 43.9 all-gather.14
  248.8 32.2 all-gather.16
  299.5 35.6 all-gather.18
  337.3 61.7 all-gather.20
  400.8 39.2 all-gather.22
  453.4 35.2 reduce-scatter.4
where the time goes:
time: 500 us; the launch traced here: 497 us
  waiting for transfers between devices  315 us (63%)
  blocking collectives  88.9 us (18%)
  matrix products  48.3 us (10%)
  starting transfers between devices  16.3 us (3%)
  other arithmetic  13.8 us (3%)
  between operations  13.8 us (3%)
    all_gather x2, waiting for transfers between devices, in_one_piece(): out = lax.all_gather(both, axis, axis=dim, tiled=True)  122 us
    all_gather x2, waiting for transfers between devices, gathered_by_axis(): out = lax.all_gather(out, axes[number], axis=dim, tiled=True)  69.1 us
    all_gather x2, waiting for transfers between devices, gather_rows(): return lax.all_gather(shard, 'tp', axis=1, tiled=True)  38.4 us
    reduce_scatter x2, waiting for transfers between devices, feed_forward(): lax.psum_scatter(partial_value.astype(jnp.bfloat16), 'tp', scatter_dimens...  35.4 us
    all_gather x2, blocking collectives, gathered_by_axis(): out = lax.all_gather(out, axes[number], axis=dim, tiled=True)  35.4 us
    dot_general x2, matrix products, feed_forward(): jnp.dot(hidden, gathered_by_axis(down_weight, FS, 1), preferred_element_t...  26.2 us
    all_gather x1, waiting for transfers between devices, per_device(): lax.all_gather(output_cols, 'tp', axis=0, tiled=True)  26 us
    all_gather x1, blocking collectives, per_device(): lax.all_gather(mix_input, FS, axis=0, tiled=True)  21 us
  transfers between devices with their start and end apart: 12, of which 11 were waited for; matrix products, arithmetic and copies ran while one was open for 6% of the time, Pallas kernels for 0%

commit v1 on v0

v1 whole, which is shorter than its diff:
```python
import functools

import jax
import jax.numpy as jnp
from jax import lax
from jax.experimental import pallas as pl
from jax.experimental.pallas import tpu as pltpu
from jax.sharding import PartitionSpec as P

EPSILON = 1e-06
CHUNKS = 4
F32 = jnp.float32
BF16 = jnp.bfloat16
VMEM_LIMIT = 66_900_000


class Task:
    def __init__(self, name, waits=(), after=(), work=None, cost=0.05, sends=(), rank=0):
        self.name, self.waits, self.after = name, list(waits), list(after)
        self.work, self.cost, self.sends, self.rank = work, cost, list(sends), rank


def ordered(tasks):
    rate = {"c": 600e3, "l": 1000e3}
    delay = {"c": 1.0, "l": 1.0}
    free, arrive, done, now, out = {}, {}, set(), 0.0, []
    left = list(tasks)
    while left:
        best = None
        for place, task in enumerate(left):
            if any(a not in done for a in task.after) or any(w not in arrive for w in task.waits):
                continue
            ready = max([0.0] + [arrive[w] for w in task.waits])
            key = (max(ready, now), task.rank, ready, place)
            if best is None or key < best[0]:
                best = (key, task)
        assert best is not None, [t.name for t in left]
        task = best[1]
        now = max(now, best[0][0]) + task.cost
        left.remove(task)
        done.add(task.name)
        out.append((now, task))
        for event, link, size, _ in task.sends:
            begin = max(now, free.get(link, 0.0))
            free[link] = begin + size / rate.get(link, 45e3)
            arrive[event] = free[link] + delay.get(link, 2.0)
    return out


def layer_kernel(
    rows_all, width, ring,
    tokens, first_gain, first_gate, first_up, first_down, mix_gain, mix_input, pool_weight, pool_scale, mix_output,
    second_gain, second_gate, second_up, second_down, out,
    gates, ups, downs, mixw, pool_w, feats, hidden, normed, part_send, part_recv, part_own, half_recv, full_recv,
    history, send_sem, recv_sem, local_sem,
):
    fs, tp = lax.axis_index("fs"), lax.axis_index("tp")
    z, y = lax.div(fs, ring), lax.rem(fs, ring)
    x, c = lax.div(tp, 2), lax.rem(tp, 2)
    other = 1 - c

    def step(value, by):
        return lax.rem(value + by + ring, ring)

    devices = {
        "y+": {"fs": z * ring + step(y, 1)}, "y-": {"fs": z * ring + step(y, -1)},
        "z+": {"fs": step(z, 1) * ring + y}, "z-": {"fs": step(z, -1) * ring + y},
        "x+": {"tp": step(x, 1) * 2 + c}, "x-": {"tp": step(x, -1) * 2 + c},
        "c": {"tp": x * 2 + other},
    }
    barrier = pltpu.get_barrier_semaphore()
    for device in devices.values():
        pl.semaphore_signal(barrier, inc=1, device_id=device, device_id_type=pl.DeviceIdType.MESH)
    pl.semaphore_wait(barrier, len(devices))

    count = [0]
    tasks = []

    def size_of(shape):
        total = 2
        for extent in shape:
            total *= extent
        return total

    def remote(event, link, make_src, make_dst, shape):
        slot = count[0]
        count[0] += 1

        def make():
            return pltpu.make_async_remote_copy(
                src_ref=make_src(), dst_ref=make_dst(), send_sem=send_sem.at[slot], recv_sem=recv_sem.at[slot],
                device_id=devices[link], device_id_type=pl.DeviceIdType.MESH,
            )

        return (event, link, size_of(shape), make)

    def same(event, link, make_ref, shape):
        return remote(event, link, make_ref, make_ref, shape)

    locals_made = [0]

    def local(event, make_src, make_dst, shape):
        slot = locals_made[0]
        locals_made[0] += 1

        def make():
            return pltpu.make_async_copy(make_src(), make_dst(), local_sem.at[slot])

        return (event, "l", size_of(shape), make)

    def gather_weights(name, buf, pieces, before):
        rows, cols = buf.shape[2], buf.shape[3]
        half, quarter = rows // 2, rows // 4
        loads = []
        for number, (src, start, length) in enumerate(pieces):
            loads.append(local(
                f"{name}l{number}", lambda src=src: src, lambda start=start, length=length: buf.at[z, y, pl.ds(start, length)],
                (length, cols),
            ))
        tasks.append(Task(f"{name}load", sends=loads, cost=0.01, rank=-2))

        def a_rows(start, length, zz):
            return buf.at[zz, :, pl.ds(start, length)]

        def b_rows(start, length, yy):
            return buf.at[:, yy, pl.ds(start, length)]

        def own(start, length, zz, yy):
            return buf.at[zz, yy, pl.ds(start, length)]

        tasks.append(Task(f"{name}1", waits=[e[0] for e in loads], after=before, sends=[
            same(f"{name}A1+", "y+", lambda: own(0, half, z, y), (half, cols)),
            same(f"{name}A1-", "y-", lambda: own(0, half, z, y), (half, cols)),
            same(f"{name}B1+", "z+", lambda: own(half, half, z, y), (half, cols)),
            same(f"{name}B1-", "z-", lambda: own(half, half, z, y), (half, cols)),
        ]))
        tasks.append(Task(f"{name}2A", waits=[f"{name}A1+", f"{name}A1-"], sends=[
            same(f"{name}A2+", "y+", lambda: own(0, quarter, z, step(y, -1)), (quarter, cols)),
            same(f"{name}A2-", "y-", lambda: own(quarter, quarter, z, step(y, 1)), (quarter, cols)),
        ]))
        tasks.append(Task(f"{name}2B", waits=[f"{name}B1+", f"{name}B1-"], sends=[
            same(f"{name}B2+", "z+", lambda: own(half, quarter, step(z, -1), y), (quarter, cols)),
            same(f"{name}B2-", "z-", lambda: own(half + quarter, quarter, step(z, 1), y), (quarter, cols)),
        ]))
        tasks.append(Task(f"{name}3A", waits=[f"{name}A2+", f"{name}A2-"], after=[f"{name}2A"], sends=[
            same(f"{name}A3+", "z+", lambda: a_rows(0, half, z), (ring, half, cols)),
            same(f"{name}A3-", "z-", lambda: a_rows(0, half, z), (ring, half, cols)),
        ]))
        tasks.append(Task(f"{name}3B", waits=[f"{name}B2+", f"{name}B2-"], after=[f"{name}2B"], sends=[
            same(f"{name}B3+", "y+", lambda: b_rows(half, half, y), (ring, half, cols)),
            same(f"{name}B3-", "y-", lambda: b_rows(half, half, y), (ring, half, cols)),
        ]))
        tasks.append(Task(f"{name}4A", waits=[f"{name}A3+", f"{name}A3-"], sends=[
            same(f"{name}A4+", "z+", lambda: a_rows(0, quarter, step(z, -1)), (ring, quarter, cols)),
            same(f"{name}A4-", "z-", lambda: a_rows(quarter, quarter, step(z, 1)), (ring, quarter, cols)),
        ]))
        tasks.append(Task(f"{name}4B", waits=[f"{name}B3+", f"{name}B3-"], sends=[
            same(f"{name}B4+", "y+", lambda: b_rows(half, quarter, step(y, -1)), (ring, quarter, cols)),
            same(f"{name}B4-", "y-", lambda: b_rows(half + quarter, quarter, step(y, 1)), (ring, quarter, cols)),
        ]))
        tasks.append(Task(f"{name}end", waits=[f"{name}A4+", f"{name}A4-", f"{name}B4+", f"{name}B4-"], rank=0, cost=0.02,
                          after=[f"{name}4A", f"{name}4B"]))

    def block_of(xx, cc):
        return xx * 2 + cc

    def send_own(buf, tag, start, length):
        def own():
            return buf.at[tp, pl.ds(start, length)]
        shape = (length, width)
        return [
            same(f"{tag}p", "x+", own, shape), same(f"{tag}m", "x-", own, shape), same(f"{tag}s0", "c", own, shape),
        ]

    def gather_features(buf, tag, start, length):
        half = length // 2

        def view(xx, begin, extent):
            return buf.at[block_of(xx, c), pl.ds(begin, extent)]

        tasks.append(Task(f"{tag}5", waits=[f"{tag}p", f"{tag}m"], sends=[
            same(f"{tag}fp", "x+", lambda: view(step(x, -1), start, half), (half, width)),
            same(f"{tag}fm", "x-", lambda: view(step(x, 1), start + half, half), (half, width)),
            same(f"{tag}s1", "c", lambda: view(step(x, -1), start, length), (length, width)),
            same(f"{tag}s2", "c", lambda: view(step(x, 1), start, length), (length, width)),
        ]))
        tasks.append(Task(f"{tag}6", waits=[f"{tag}fp", f"{tag}fm"], after=[f"{tag}5"], sends=[
            same(f"{tag}s3", "c", lambda: view(step(x, 2), start, length), (length, width)),
        ]))
        return dict(waits=[f"{tag}s{n}" for n in range(4)], after=[f"{tag}6"])

    def scatter_sums(stage, tag, start, length, before, finish):
        rows = pl.ds(start, length)
        half = length // 2
        low, high = pl.ds(start, half), pl.ds(start + half, half)
        at = stage % 2
        mid = lax.rem
        far, right, left = step(x, 2), step(x, 1), step(x, -1)
        compact = pl.ds(start // 2, half)

        def fold_far():
            total = part_own[at, far, rows].astype(F32) + part_recv[stage, far, rows].astype(F32)
            part_own[at, far, rows] = total.astype(BF16)

        tasks.append(Task(f"{tag}2", waits=[f"{tag}sib"], after=before, work=fold_far, cost=0.2, sends=[
            remote(f"{tag}hp", "x+", lambda: part_own.at[at, far, low], lambda: half_recv.at[stage, 0, compact], (half, width)),
            remote(f"{tag}hm", "x-", lambda: part_own.at[at, far, high], lambda: half_recv.at[stage, 1, compact], (half, width)),
        ]))

        def fold_near():
            for target, extra, plain, number in ((right, low, high, 0), (left, high, low, 1)):
                total = part_own[at, target, extra].astype(F32) + part_recv[stage, target, extra].astype(F32)
                total = total + half_recv[stage, number, compact].astype(F32)
                part_own[at, target, extra] = total.astype(BF16)
                total = part_own[at, target, plain].astype(F32) + part_recv[stage, target, plain].astype(F32)
                part_own[at, target, plain] = total.astype(BF16)

        tasks.append(Task(f"{tag}3", waits=[f"{tag}hp", f"{tag}hm"], after=[f"{tag}2"], work=fold_near, cost=0.3, sends=[
            remote(f"{tag}dp", "x+", lambda: part_own.at[at, right, rows], lambda: full_recv.at[stage, 0, rows], (length, width)),
            remote(f"{tag}dm", "x-", lambda: part_own.at[at, left, rows], lambda: full_recv.at[stage, 1, rows], (length, width)),
        ]))

        def total_rows():
            total = part_own[at, x, rows].astype(F32) + part_recv[stage, x, rows].astype(F32)
            return total + full_recv[stage, 0, rows].astype(F32) + full_recv[stage, 1, rows].astype(F32)

        work, sends = finish(total_rows)
        tasks.append(Task(f"{tag}4", waits=[f"{tag}dp", f"{tag}dm"], after=[f"{tag}3"], work=work, cost=0.3, sends=sends))

    def send_parts(stage, tag, start, length):
        rows = pl.ds(start, length)
        return [remote(
            f"{tag}sib", "c", lambda: part_send.at[stage % 2, :, rows], lambda: part_recv.at[stage, :, rows],
            (ring, length, width),
        )]

    def normalize_rows(stage, gain, start, length):
        sub = 16
        gains = [gain[:, b * width:(b + 1) * width] for b in range(2 * ring)]

        def body(i, carry):
            base = pl.multiple_of(start + i * sub, sub)
            values = [feats[stage, b, pl.ds(base, sub), :].astype(F32) for b in range(2 * ring)]
            squares = functools.reduce(lambda a, b: a + b, [v * v for v in values])
            mean = jnp.sum(squares, axis=-1, keepdims=True) * (1.0 / (2 * ring * width))
            factor = lax.rsqrt(mean + EPSILON)
            for b, v in enumerate(values):
                normed[pl.ds(pl.multiple_of(i * sub, sub), sub), b * width:(b + 1) * width] = (
                    v * factor * gains[b]
                ).astype(BF16)
            return carry

        lax.fori_loop(0, length // sub, body, 0, unroll=2)

    tile = 256

    def hidden_rows(which, stage, gain, start, length):
        def work():
            normalize_rows(stage, gain, start, length)
            depth = 2 * ring * width

            def body(n, carry):
                cols = pl.ds(pl.multiple_of(n * tile, tile), tile)
                gate_w = gates[which, :, :, :, cols].reshape(depth, tile)
                up_w = ups[which, :, :, :, cols].reshape(depth, tile)
                both = jnp.dot(
                    normed[0:length, :], jnp.concatenate([gate_w, up_w], axis=1), preferred_element_type=F32
                )
                gated, upward = both[:, :tile], both[:, tile:]
                value = gated / (1.0 + jnp.exp(-gated)) * upward
                hidden[pl.ds(start, length), cols] = value.astype(BF16)
                return carry

            lax.fori_loop(0, hidden.shape[1] // tile, body, 0)
        return work

    def product_rows(left_value, weight_of, target, slot, side, start, length):
        def body(pair, carry):
            columns = []
            for j in range(2):
                block = block_of(pair * 2 + j, side) * 2
                for k in range(2):
                    index = block + k
                    columns.append(weight_of(lax.div(index, ring), lax.rem(index, ring)))
            value = jnp.dot(left_value(), jnp.concatenate(columns, axis=1), preferred_element_type=F32)
            for j in range(2):
                target[slot, pair * 2 + j, pl.ds(start, length)] = value[:, j * width:(j + 1) * width].astype(BF16)
            return carry

        lax.fori_loop(0, ring // 2, body, 0)

    def down_rows(which, stage, target, side, start, length):
        def work():
            product_rows(
                lambda: hidden[pl.ds(start, length), :], lambda zz, yy: downs[which, zz, yy], target, stage % 2, side,
                start, length,
            )
        return work

    pad = 16

    def pool_rows(start, length):
        def work():
            normalize_rows(1, mix_gain, start, length)
            weight = mixw[:, :, 0:128, :].reshape(2 * ring * width, 128)
            pool_in = jnp.dot(normed[0:length, :], weight, preferred_element_type=F32).astype(BF16).astype(F32)
            if start == 0:
                history[0:pad, :] = jnp.zeros((pad, 128), F32)
            history[pl.ds(pad + start, length), :] = pool_in
            span = history[pl.ds(start, length + pad), :]
            sums = []
            for shift in (1, 2, 4, 8):
                span = span + pltpu.roll(span, shift, 0)
                sums.append(span[pad:, :])
            window = jnp.left_shift(jnp.int32(2), lax.rem(tp, 4))
            total = jnp.where(window == 2, sums[0], jnp.where(window == 4, sums[1], jnp.where(window == 8, sums[2], sums[3])))
            position = start + lax.broadcasted_iota(jnp.int32, (length, 128), 0)
            number = jnp.minimum(position + 1, window).astype(F32)
            pooled = (total / number - pool_in).astype(BF16)
            mapped = jnp.dot(pooled, pool_w[...], preferred_element_type=F32)
            hidden[pl.ds(start, length), 0:128] = (mapped * pool_scale[pl.ds(tp, 1), :]).astype(BF16)
        return work

    def mix_rows(target, side, start, length):
        def work():
            product_rows(
                lambda: hidden[pl.ds(start, length), 0:128], lambda zz, yy: mixw[zz, yy, 128:256, :], target, 1, side,
                start, length,
            )
        return work

    items = [
        ("g1", gates.at[0], [(first_gate, 0, 128)]), ("u1", ups.at[0], [(first_up, 0, 128)]),
        ("d1", downs.at[0], [(first_down, 0, downs.shape[3])]),
        ("mx", mixw, [(mix_input, 0, 128), (mix_output, 128, 128)]),
        ("g2", gates.at[1], [(second_gate, 0, 128)]), ("u2", ups.at[1], [(second_up, 0, 128)]),
        ("d2", downs.at[1], [(second_down, 0, downs.shape[3])]),
    ]
    token_load = local("tok", lambda: tokens, lambda: feats.at[0, tp], (rows_all, width))
    tasks.append(Task("tokload", sends=[token_load], cost=0.01, rank=-3))
    for number, (name, buf, pieces) in enumerate(items):
        before = [f"{items[number - 2][0]}3A", f"{items[number - 2][0]}3B"] if number >= 2 else []
        gather_weights(name, buf, pieces, before)
    tasks.append(Task("poolload", cost=0.01, sends=[local("pw", lambda: pool_weight.at[tp], lambda: pool_w, (128, 128))]))
    tasks.append(Task("tok1", waits=["tok"], sends=send_own(feats.at[0], "t0", 0, rows_all)))
    seen = gather_features(feats.at[0], "t0", 0, rows_all)
    tasks.append(Task("tokend", cost=0.01, **seen))

    length = rows_all // CHUNKS
    for k in range(CHUNKS):
        start = k * length
        rows = pl.ds(start, length)
        tasks.append(Task(f"h1{k}", after=["tokend", "g1end", "u1end"] + ([f"h1{k - 1}"] if k else []),
                          work=hidden_rows(0, 0, first_gain, start, length), cost=2.5, rank=2))
        tasks.append(Task(f"ps0{k}", after=[f"h1{k}", "d1end"], work=down_rows(0, 0, part_send, other, start, length),
                          cost=0.6, rank=1, sends=send_parts(0, f"r0{k}", start, length)))
        tasks.append(Task(f"po0{k}", after=[f"ps0{k}"], work=down_rows(0, 0, part_own, c, start, length), cost=0.6, rank=1))

        def finish_first(total_rows, start=start, rows=rows, k=k):
            def work():
                value = feats[0, tp, rows].astype(F32) + 0.5 * total_rows()
                feats[1, tp, rows] = value.astype(BF16)
            return work, send_own(feats.at[1], f"m{k}", start, length)

        scatter_sums(0, f"r0{k}", start, length, [f"po0{k}"], finish_first)
        seen = gather_features(feats.at[1], f"m{k}", start, length)
        tasks.append(Task(f"pool{k}", waits=seen["waits"] + (["pw"] if k == 0 else []),
                          after=seen["after"] + ["mxend"] + ([f"pool{k - 1}"] if k else []),
                          work=pool_rows(start, length), cost=1.2, rank=1))
        tasks.append(Task(f"ps1{k}", after=[f"pool{k}"], work=mix_rows(part_send, other, start, length),
                          cost=0.3, rank=1, sends=send_parts(1, f"r1{k}", start, length)))
        tasks.append(Task(f"po1{k}", after=[f"ps1{k}"], work=mix_rows(part_own, c, start, length), cost=0.3, rank=1))

        def finish_mixer(total_rows, start=start, rows=rows, k=k):
            def work():
                value = feats[1, tp, rows].astype(F32) + total_rows()
                feats[2, tp, rows] = value.astype(BF16)
            return work, send_own(feats.at[2], f"n{k}", start, length)

        scatter_sums(1, f"r1{k}", start, length, [f"po1{k}"], finish_mixer)
        seen = gather_features(feats.at[2], f"n{k}", start, length)
        reuse = [f"send:r0{k}sib", f"send:r0{k}hp", f"send:r0{k}hm", f"send:r0{k}dp", f"send:r0{k}dm"]
        tasks.append(Task(f"h2{k}", waits=seen["waits"], after=seen["after"] + ["g2end", "u2end", f"ps1{k}", f"po1{k}"],
                          work=hidden_rows(1, 2, second_gain, start, length), cost=2.5, rank=2))
        tasks.append(Task(f"ps2{k}", after=[f"h2{k}", "d2end", f"r0{k}4"], work=down_rows(1, 2, part_send, other, start, length),
                          cost=0.6, rank=1, sends=send_parts(2, f"r2{k}", start, length)))
        tasks[-1].reuse = reuse
        tasks.append(Task(f"po2{k}", after=[f"ps2{k}"], work=down_rows(1, 2, part_own, c, start, length), cost=0.6, rank=1))

        def finish_second(total_rows, rows=rows):
            def work():
                value = feats[2, tp, rows].astype(F32) + 0.5 * total_rows()
                out[rows, :] = value.astype(BF16)
            return work, []

        scatter_sums(2, f"r2{k}", start, length, [f"po2{k}"], finish_second)

    order = ordered(tasks)
    if False:
        for moment, task in order:
            print(f"{moment:8.2f} {task.name}")
    events, sent, waited = {}, {}, set()
    for _, task in order:
        for event in getattr(task, "reuse", []):
            name = event[5:]
            sent.pop(name).wait_send()
        for event in task.waits:
            copy = events[event]
            if isinstance(copy, tuple):
                copy[0].wait()
            else:
                copy.wait_recv()
            waited.add(event)
        if task.work is not None:
            task.work()
        for event, link, _, make in task.sends:
            copy = make()
            copy.start()
            if link == "l":
                events[event] = (copy,)
            else:
                events[event] = copy
                sent[event] = copy
    assert waited == set(events)
    for copy in sent.values():
        copy.wait_send()
    assert count[0] <= send_sem.shape[0] and locals_made[0] <= local_sem.shape[0], (count[0], locals_made[0])


def per_device(
    tokens, first_gain, first_gate, first_up, first_down, mix_gain, mix_input, pool_weight, pool_scale, mix_output,
    second_gain, second_gate, second_up, second_down, *, ring,
):
    rows, width = tokens.shape
    units = first_gate.shape[1]
    model = first_gain.shape[0]
    remote_copies, local_copies = 7 * 16 + 8 + CHUNKS * 31, 10
    flat = lambda gain: gain.reshape(1, model)
    anywhere = pl.BlockSpec(memory_space=pl.ANY)
    inside = pl.BlockSpec(memory_space=pltpu.VMEM)
    scratch = [
        pltpu.VMEM((2, ring, ring, 128, units), BF16),
        pltpu.VMEM((2, ring, ring, 128, units), BF16),
        pltpu.VMEM((2, ring, ring, units, 128), BF16),
        pltpu.VMEM((ring, ring, 256, 128), BF16),
        pltpu.VMEM((128, 128), BF16),
        pltpu.VMEM((3, 2 * ring, rows, width), BF16),
        pltpu.VMEM((rows, units), BF16),
        pltpu.VMEM((rows // CHUNKS, model), BF16),
        pltpu.VMEM((2, ring, rows, width), BF16),
        pltpu.VMEM((3, ring, rows, width), BF16),
        pltpu.VMEM((2, ring, rows, width), BF16),
        pltpu.VMEM((3, 2, rows // 2, width), BF16),
        pltpu.VMEM((3, 2, rows, width), BF16),
        pltpu.VMEM((rows + 16, 128), F32),
        pltpu.SemaphoreType.DMA((remote_copies,)),
        pltpu.SemaphoreType.DMA((remote_copies,)),
        pltpu.SemaphoreType.DMA((local_copies,)),
    ]
    return pl.pallas_call(
        functools.partial(layer_kernel, rows, width, ring),
        out_shape=jax.ShapeDtypeStruct((rows, width), BF16),
        in_specs=[
            anywhere, inside, anywhere, anywhere, anywhere, inside, anywhere, anywhere, inside, anywhere,
            inside, anywhere, anywhere, anywhere,
        ],
        out_specs=inside,
        scratch_shapes=scratch,
        compiler_params=pltpu.CompilerParams(collective_id=0, has_side_effects=True, vmem_limit_bytes=VMEM_LIMIT),
    )(
        tokens, flat(first_gain), first_gate, first_up, first_down, flat(mix_gain), mix_input, pool_weight,
        pool_scale.reshape(-1, 128), mix_output, flat(second_gain), second_gate, second_up, second_down,
    )


def solution(mesh):
    weight, turned = P("fs", "tp"), P("tp", "fs")
    return jax.shard_map(
        functools.partial(per_device, ring=mesh.shape["tp"] // 2),
        mesh=mesh,
        in_specs=(
            P("fs", "tp"), P(), weight, weight, turned, P(), weight, P(), P(), turned, P(), weight, weight, turned,
        ),
        out_specs=P("fs", "tp"),
        check_vma=False,
    )
```

time: 500 us -> 182 us (0.36)
  waiting for transfers between devices: 315 us -> 0 us
  Pallas kernels: 0 us -> 179 us
  blocking collectives: 88.9 us -> 0 us
  matrix products: 48.3 us -> 0 us
  starting transfers between devices: 16.3 us -> 0 us
  other arithmetic: 13.8 us -> 0 us
  between operations: 13.8 us -> 0.01 us
    all_gather x8 -> x0, waiting for transfers between devices: 263 us -> none  [the longest x2 122 us: in_one_piece(): out = lax.all_gather(both, axis, axis=dim, tiled=True)]
    pallas_call x0 -> x1, Pallas kernels: none -> 179 us  [per_device(): pl.pallas_call(functools.partial(layer_kernel, rows, width, ring), out_sh...]
    all_gather x4 -> x0, blocking collectives: 76.5 us -> none  [the longest x2 35.4 us: gathered_by_axis(): out = lax.all_gather(out, axes[number], axis=dim, tiled=True)]
    dot_general x14 -> x0, matrix products: 48.3 us -> none  [the longest x2 26.2 us: feed_forward(): jnp.dot(hidden, gathered_by_axis(down_weight, FS, 1), preferred_element_t...]
    reduce_scatter x2 -> x0, waiting for transfers between devices: 35.4 us -> none  [feed_forward(): lax.psum_scatter(partial_value.astype(jnp.bfloat16), 'tp', scatter_dimens...]
    all_to_all x1 -> x0, waiting for transfers between devices: 14.2 us -> none  [per_device(): lax.all_to_all(first_out, 'tp', split_axis=0, concat_axis=1, tiled=True)]
    all_to_all x1 -> x0, starting transfers between devices: 13.9 us -> none  [per_device(): lax.all_to_all(first_out, 'tp', split_axis=0, concat_axis=1, tiled=True)]
    all_to_all x1 -> x0, blocking collectives: 12.3 us -> none  [per_device(): lax.all_to_all(result.astype(jnp.bfloat16), 'tp', split_axis=1, concat_ax...]
  transfers between devices with their start and end apart: 12 -> 0, of which waited for: 11 -> 0; matrix products, arithmetic and copies ran while one was open for 6% -> 0% of each run, Pallas kernels for 0% -> 0%
where the time goes in v1:
time: 182 us; the launch traced here: 181 us
  Pallas kernels  179 us (98%)
  local copies, waits for them, and re-layouts  1.87 us (1%)
    pallas_call x1, Pallas kernels, per_device(): pl.pallas_call(functools.partial(layer_kernel, rows, width, ring), out_sh...  179 us

profile of v1, /device:TPU:1, one launch (start us, length us, event | category | flops | bytes accessed | tf_op | source)
XLA Modules:
  0.0 181.4 jit_solution(9228084909897674641)
XLA Ops:
  0.0 179.5 %shard_map.136 = bf16[1024,256]{1,0:T(8,128)(2,1)} custom-call(bf16[1024,256]{1,0:T(8,128)(2,1)} %tokens.1, f32[1,2048]{1,0:T(1,128)} %bitcast.4, bf16[128,768]{1,0:T(8,128)(2,1)} %first_gate.1, bf16[128,768]{1,0:T(8,128)(2,1)} %first_up.1, bf16[768,128]{1,0:T(8,128)(2,1)} %first_down.1, f32[1,2048]{1,0:T(1,128)} %bitcast.5, bf16[128,128]{1,0:T(8,128)(2,1)} %mix_input.1, ...), custom_call_target="tpu_custom_call" | custom-call | tf_op jit(solution)/shard_map/pallas_call | solution.py:460
  179.5 1.9 %copy.16 = bf16[1024,256]{1,0:T(8,128)(2,1)} copy(bf16[1024,256]{1,0:T(8,128)(2,1)} %shard_map.136) | data formatting | bytes 1048576

commit v2 on v1

v2 whole, which is shorter than its diff:
```python
import functools

import jax
import jax.numpy as jnp
from jax import lax
from jax.experimental import pallas as pl
from jax.experimental.pallas import tpu as pltpu
from jax.sharding import PartitionSpec as P

EPSILON = 1e-06
CHUNKS = 4
HALO = 16
F32 = jnp.float32
BF16 = jnp.bfloat16
VMEM_LIMIT = 66_900_000
MESH = pl.DeviceIdType.MESH


class Task:
    def __init__(self, name, waits=(), after=(), work=None, cost=0.05, sends=(), rank=0):
        self.name, self.waits, self.after = name, list(waits), list(after)
        self.work, self.cost, self.sends, self.rank = work, cost, list(sends), rank


def ordered(tasks):
    rate = {"c": 600e3, "l": 1000e3}
    delay = {"c": 1.0, "l": 1.0}
    free, arrive, done, now, out = {}, {}, set(), 0.0, []
    left = list(tasks)
    while left:
        best = None
        for place, task in enumerate(left):
            if any(a not in done for a in task.after) or any(w not in arrive for w in task.waits):
                continue
            ready = max([0.0] + [arrive[w] for w in task.waits])
            key = (max(ready, now), task.rank, ready, place)
            if best is None or key < best[0]:
                best = (key, task)
        assert best is not None, [t.name for t in left]
        task = best[1]
        now = max(now, best[0][0]) + task.cost
        left.remove(task)
        done.add(task.name)
        out.append((now, task))
        for event, link, size, _ in task.sends:
            route = link[:2] if link[0] in "xyz" else link[0]
            begin = max(now, free.get(route, 0.0))
            free[route] = begin + size / rate.get(route, 45e3)
            arrive[event] = free[route] + delay.get(route, 2.0)
    return out


def build(ring, fs, tp, refs):
    (
        tokens, first_gain, first_gate, first_up, first_down, mix_gain, mix_input, pool_weight, pool_scale, mix_output,
        second_gain, second_gate, second_up, second_down, out,
        gates, ups, downs, mixw, feats, middle, hidden, normed, run_normed, first_run, pool_in, halo, mapped_run,
        rows_part, rows_sib, rows_half, rows_full, cols_part, cols_sib, cols_half, cols_full,
        send_sem, recv_sem, local_sem,
    ) = refs
    z, y = lax.div(fs, ring), lax.rem(fs, ring)
    x, c = lax.div(tp, 2), lax.rem(tp, 2)
    other = 1 - c
    blocks = 2 * ring
    rows_all, width = tokens.shape
    model = blocks * width
    length = rows_all // CHUNKS
    run = length // blocks
    lane = 128

    def step(value, by):
        return lax.rem(value + by + ring, ring)

    devices = {
        "y+": {"fs": z * ring + step(y, 1)}, "y-": {"fs": z * ring + step(y, -1)},
        "z+": {"fs": step(z, 1) * ring + y}, "z-": {"fs": step(z, -1) * ring + y},
        "x+": {"tp": step(x, 1) * 2 + c}, "x-": {"tp": step(x, -1) * 2 + c},
        "c": {"tp": x * 2 + other},
        "next": {"tp": lax.rem(tp + 1, blocks)}, "last": {"tp": lax.rem(tp + blocks - 1, blocks)},
    }
    tasks, counts = [], {"r": 0, "l": 0}

    def add(*args, **kwargs):
        tasks.append(Task(*args, **kwargs))

    def size_of(shape):
        total = 2
        for extent in shape:
            total *= extent
        return total

    def remote(event, link, make_src, make_dst, shape):
        slot = counts["r"]
        counts["r"] += 1

        def make():
            return pltpu.make_async_remote_copy(
                src_ref=make_src(), dst_ref=make_dst(), send_sem=send_sem.at[slot], recv_sem=recv_sem.at[slot],
                device_id=devices[link], device_id_type=MESH,
            )

        return (event, "x+" if link == "next" else link, size_of(shape), make)

    def same(event, link, make_ref, shape):
        return remote(event, link, make_ref, make_ref, shape)

    def local(event, make_src, make_dst, shape):
        slot = counts["l"]
        counts["l"] += 1
        return (event, "l", size_of(shape), lambda: pltpu.make_async_copy(make_src(), make_dst(), local_sem.at[slot]))

    def gather_weights(name, buf, pieces, before):
        rows, cols = buf.shape[2], buf.shape[3]
        half, quarter = rows // 2, rows // 4
        loads = [
            local(
                f"{name}l{number}", lambda src=src: src,
                lambda start=start, extent=extent: buf.at[z, y, pl.ds(start, extent)], (extent, cols),
            )
            for number, (src, start, extent) in enumerate(pieces)
        ]
        add(f"{name}load", sends=loads, cost=0.01, rank=-2)

        def a_rows(start, extent, zz):
            return buf.at[zz, :, pl.ds(start, extent)]

        def b_rows(start, extent, yy):
            return buf.at[:, yy, pl.ds(start, extent)]

        def own(start, extent, zz, yy):
            return buf.at[zz, yy, pl.ds(start, extent)]

        add(f"{name}1", waits=[e[0] for e in loads], after=before, sends=[
            same(f"{name}A1+", "y+", lambda: own(0, half, z, y), (half, cols)),
            same(f"{name}A1-", "y-", lambda: own(0, half, z, y), (half, cols)),
            same(f"{name}B1+", "z+", lambda: own(half, half, z, y), (half, cols)),
            same(f"{name}B1-", "z-", lambda: own(half, half, z, y), (half, cols)),
        ])
        add(f"{name}2A", waits=[f"{name}A1+", f"{name}A1-"], sends=[
            same(f"{name}A2+", "y+", lambda: own(0, quarter, z, step(y, -1)), (quarter, cols)),
            same(f"{name}A2-", "y-", lambda: own(quarter, quarter, z, step(y, 1)), (quarter, cols)),
        ])
        add(f"{name}2B", waits=[f"{name}B1+", f"{name}B1-"], sends=[
            same(f"{name}B2+", "z+", lambda: own(half, quarter, step(z, -1), y), (quarter, cols)),
            same(f"{name}B2-", "z-", lambda: own(half + quarter, quarter, step(z, 1), y), (quarter, cols)),
        ])
        add(f"{name}3A", waits=[f"{name}A2+", f"{name}A2-"], after=[f"{name}2A"], sends=[
            same(f"{name}A3+", "z+", lambda: a_rows(0, half, z), (ring, half, cols)),
            same(f"{name}A3-", "z-", lambda: a_rows(0, half, z), (ring, half, cols)),
        ])
        add(f"{name}3B", waits=[f"{name}B2+", f"{name}B2-"], after=[f"{name}2B"], sends=[
            same(f"{name}B3+", "y+", lambda: b_rows(half, half, y), (ring, half, cols)),
            same(f"{name}B3-", "y-", lambda: b_rows(half, half, y), (ring, half, cols)),
        ])
        add(f"{name}4A", waits=[f"{name}A3+", f"{name}A3-"], sends=[
            same(f"{name}A4+", "z+", lambda: a_rows(0, quarter, step(z, -1)), (ring, quarter, cols)),
            same(f"{name}A4-", "z-", lambda: a_rows(quarter, quarter, step(z, 1)), (ring, quarter, cols)),
        ])
        add(f"{name}4B", waits=[f"{name}B3+", f"{name}B3-"], sends=[
            same(f"{name}B4+", "y+", lambda: b_rows(half, quarter, step(y, -1)), (ring, quarter, cols)),
            same(f"{name}B4-", "y-", lambda: b_rows(half + quarter, quarter, step(y, 1)), (ring, quarter, cols)),
        ])
        add(f"{name}endA", waits=[f"{name}A4+", f"{name}A4-"], cost=0.02, after=[f"{name}4A"])
        add(f"{name}endB", waits=[f"{name}B4+", f"{name}B4-"], cost=0.02, after=[f"{name}4B"])

    def ends(*names):
        return [f"{name}end{half}" for name in names for half in "AB"]

    def block_of(xx, cc):
        return xx * 2 + cc

    def send_own(tag, view, size):
        def own():
            return view(tp, 2)
        return [
            same(f"{tag}p", "x+", own, (size,)), same(f"{tag}m", "x-", own, (size,)), same(f"{tag}s0", "c", own, (size,)),
        ]

    def gather_blocks(tag, view, size):
        def at(by, part):
            return view(block_of(step(x, by), c), part)

        add(f"{tag}5", waits=[f"{tag}p", f"{tag}m"], sends=[
            same(f"{tag}fp", "x+", lambda: at(-1, 0), (size // 2,)),
            same(f"{tag}fm", "x-", lambda: at(1, 1), (size // 2,)),
            same(f"{tag}s1", "c", lambda: at(-1, 2), (size,)),
            same(f"{tag}s2", "c", lambda: at(1, 2), (size,)),
        ])
        add(f"{tag}6", waits=[f"{tag}fp", f"{tag}fm"], after=[f"{tag}5"], sends=[
            same(f"{tag}s3", "c", lambda: at(2, 2), (size,)),
        ])
        return dict(waits=[f"{tag}s{n}" for n in range(4)], after=[f"{tag}6"])

    def scatter_sums(tag, bufs, start, extent, before, finish):
        part, sib, half_recv, full_recv = bufs
        cols = part.shape[3]
        rows, half = pl.ds(start, extent), extent // 2
        low, high, compact = pl.ds(start, half), pl.ds(start + half, half), pl.ds(start // 2, half)
        far, right, left = step(x, 2), step(x, 1), step(x, -1)

        def pair(target, which):
            return part[target, c, which].astype(F32) + sib[target, which].astype(F32)

        def fold_far():
            part[far, c, rows] = pair(far, rows).astype(BF16)

        add(f"{tag}2", waits=[f"{tag}sib"], after=before, work=fold_far, cost=0.2, sends=[
            remote(f"{tag}hp", "x+", lambda: part.at[far, c, low], lambda: half_recv.at[0, compact], (half, cols)),
            remote(f"{tag}hm", "x-", lambda: part.at[far, c, high], lambda: half_recv.at[1, compact], (half, cols)),
        ])

        def fold_near():
            for target, extra, plain, number in ((right, low, high, 0), (left, high, low, 1)):
                part[target, c, extra] = (pair(target, extra) + half_recv[number, compact].astype(F32)).astype(BF16)
                part[target, c, plain] = pair(target, plain).astype(BF16)

        add(f"{tag}3", waits=[f"{tag}hp", f"{tag}hm"], after=[f"{tag}2"], work=fold_near, cost=0.3, sends=[
            remote(f"{tag}dp", "x+", lambda: part.at[right, c, rows], lambda: full_recv.at[0, rows], (extent, cols)),
            remote(f"{tag}dm", "x-", lambda: part.at[left, c, rows], lambda: full_recv.at[1, rows], (extent, cols)),
        ])

        def total(span):
            return (
                part[x, c, rows, span].astype(F32) + sib[x, rows, span].astype(F32)
                + full_recv[0, rows, span].astype(F32) + full_recv[1, rows, span].astype(F32)
            )

        work, sends, cost = finish(total)
        add(f"{tag}4", waits=[f"{tag}dp", f"{tag}dm"], after=[f"{tag}3"], work=work, cost=cost, sends=sends)

    def send_parts(tag, bufs, start, extent):
        part, sib = bufs[:2]
        rows = pl.ds(start, extent)
        return [remote(
            f"{tag}sib", "c", lambda: part.at[:, other, rows], lambda: sib.at[:, rows], (ring, extent, part.shape[3]),
        )]

    sub = 16

    def scaled(values, gains):
        squares = functools.reduce(lambda a, b: a + b, [v * v for v in values])
        mean = jnp.sum(squares, axis=-1, keepdims=True) * (1.0 / model)
        factor = lax.rsqrt(mean + EPSILON)
        return [(v * factor * g).astype(BF16) for v, g in zip(values, gains)]

    def normalize_rows(read, gain, start):
        def body(i, carry):
            base = pl.multiple_of(start + i * sub, sub)
            gains = [gain[:, b * width:(b + 1) * width] for b in range(blocks)]
            for b, v in enumerate(scaled([read(b, pl.ds(base, sub)).astype(F32) for b in range(blocks)], gains)):
                normed[pl.ds(base, sub), b * width:(b + 1) * width] = v
            return carry

        lax.fori_loop(0, length // sub, body, 0, unroll=2)

    tile = 256

    def hidden_rows(which, start):
        def work():
            def body(n, carry):
                cols = pl.ds(pl.multiple_of(n * tile, tile), tile)
                gate_w = gates[which, :, :, :, cols].reshape(model, tile)
                up_w = ups[which, :, :, :, cols].reshape(model, tile)
                both = jnp.dot(
                    normed[pl.ds(start, length), :], jnp.concatenate([gate_w, up_w], axis=1),
                    preferred_element_type=F32,
                )
                gated, upward = both[:, :tile], both[:, tile:]
                value = gated / (1.0 + jnp.exp(-gated)) * upward
                hidden[pl.ds(start, length), cols] = value.astype(BF16)
                return carry

            lax.fori_loop(0, hidden.shape[1] // tile, body, 0)
        return work

    def down_rows(which, start, store):
        def work():
            def body(n, carry):
                columns = [downs[which, n, i] for i in range(ring)]
                value = jnp.dot(
                    hidden[pl.ds(start, length), :], jnp.concatenate(columns, axis=1), preferred_element_type=F32
                )
                store(n, value.astype(BF16))
                return carry

            lax.fori_loop(0, ring, body, 0)
        return work

    wide = ring * lane

    def first_finish(k):
        start = k * length

        def finish(total):
            def work():
                place = pl.ds(pl.multiple_of(start + tp * run, run), run)
                for b in range(blocks):
                    span = slice(b * width, (b + 1) * width)
                    value = feats[b, place, :].astype(F32) + 0.5 * total(span)
                    first_run[k * run:(k + 1) * run, span] = value.astype(BF16)
            return work, [], 0.4
        return finish

    def pool_in_rows(k):
        def work():
            gains = [mix_gain[:, b * width:(b + 1) * width] for b in range(blocks)]
            for base in range(0, run, sub):
                rows = pl.ds(k * run + base, sub)
                spans = [slice(b * width, (b + 1) * width) for b in range(blocks)]
                for span, v in zip(spans, scaled([first_run[rows, span].astype(F32) for span in spans], gains)):
                    run_normed[base:base + sub, span] = v

            def body(n, carry):
                columns = [mixw[n * ring + i, :, :, 0:lane, :].reshape(model, lane) for i in range(ring)]
                value = jnp.dot(run_normed[...], jnp.concatenate(columns, axis=1), preferred_element_type=F32)
                pool_in[k, :, pl.ds(pl.multiple_of(n * wide, wide), wide)] = value.astype(BF16)
                return carry

            lax.fori_loop(0, blocks // ring, body, 0)
            if k == 0:
                halo[0] = jnp.zeros(halo.shape[1:], BF16)
        return work

    def mixer_rows(k):
        start = k * length

        def work():
            position = start + tp * run + lax.broadcasted_iota(jnp.int32, (run, lane), 0)
            slot = k + jnp.minimum(tp, 1)
            for b in range(blocks):
                span = slice(b * lane, (b + 1) * lane)
                window = 2 << (b % 4)
                current = pool_in[k, :, span].astype(F32)
                total = jnp.concatenate([halo[slot, :, span].astype(F32), current], axis=0)
                shift = 1
                while shift < window:
                    total = total + pltpu.roll(total, shift, 0)
                    shift *= 2
                number = jnp.minimum(position + 1, window).astype(F32)
                pooled = (total[HALO:, :] / number - current).astype(BF16)
                mapped = jnp.dot(pooled, pool_weight[b], preferred_element_type=F32)
                mapped_run[:, span] = (mapped * pool_scale[b:b + 1, :]).astype(BF16)
            place = pl.ds(pl.multiple_of(start + tp * run, run), run)

            def body(n, carry):
                columns = [mixw[:, n, i, lane:2 * lane, :].reshape(blocks * lane, lane) for i in range(ring)]
                value = jnp.dot(mapped_run[...], jnp.concatenate(columns, axis=1), preferred_element_type=F32)
                cols = pl.ds(pl.multiple_of(n * wide, wide), wide)
                value = first_run[k * run:(k + 1) * run, cols].astype(F32) + value
                middle[place, cols] = value.astype(BF16)
                return carry

            lax.fori_loop(0, ring, body, 0)
        return work

    units = downs.shape[3]
    items = [
        ("g1", gates.at[0], [(first_gate, 0, lane)]), ("u1", ups.at[0], [(first_up, 0, lane)]),
        ("mx", mixw.at[tp], [(mix_input, 0, lane), (mix_output, lane, lane)]),
        ("d1", downs.at[0], [(first_down, 0, units)]),
        ("g2", gates.at[1], [(second_gate, 0, lane)]), ("u2", ups.at[1], [(second_up, 0, lane)]),
        ("d2", downs.at[1], [(second_down, 0, units)]),
    ]
    token_load = local("tok", lambda: tokens, lambda: feats.at[0 + tp], (rows_all, width))
    add("tokload", sends=[token_load], cost=0.01, rank=-3)
    for number, (name, buf, pieces) in enumerate(items):
        before = [f"{items[number - 2][0]}3A", f"{items[number - 2][0]}3B"] if number >= 2 else []
        gather_weights(name, buf, pieces, before)

    def token_view(block, part):
        half = rows_all // 2
        return feats.at[block, pl.ds(*((0, half), (half, half), (0, rows_all))[part])]

    add("tok1", waits=["tok"], sends=send_own("t", token_view, rows_all * width))
    add("tokend", cost=0.01, **gather_blocks("t", token_view, rows_all * width))
    for tag, begin, half_name in (("xi", 0, "A"), ("xo", lane, "B")):
        def mix_view(block, part, begin=begin):
            half = ring // 2
            return mixw.at[block, pl.ds(*((0, half), (half, half), (0, ring))[part]), :, pl.ds(begin, lane)]

        size = ring * ring * lane * lane
        add(f"{tag}1", after=[f"mxend{half_name}"], sends=send_own(tag, mix_view, size))
        add(f"{tag}end", cost=0.01, **gather_blocks(tag, mix_view, size))

    by_rows = (rows_part, rows_sib, rows_half, rows_full)
    by_cols = (cols_part, cols_sib, cols_half, cols_full)
    for k in range(CHUNKS):
        start = k * length
        rows = pl.ds(start, length)
        before = [f"m{k - 1}"] if k else []
        add(f"n1{k}", after=["tokend"], cost=0.8, rank=3,
            work=functools.partial(normalize_rows, lambda b, place: feats[b, place, :], first_gain, start))
        add(f"h1{k}", after=[f"n1{k}"] + ends("g1", "u1"), work=hidden_rows(0, start), cost=2.0, rank=2)

        def store_rows(n, value, k=k):
            cols = pl.ds(pl.multiple_of(n * wide, wide), wide)
            for b in range(blocks):
                rows_part[b // 2, b % 2, k * run:(k + 1) * run, cols] = value[b * run:(b + 1) * run, :]

        add(f"p1{k}", after=[f"h1{k}"] + ends("d1"), work=down_rows(0, start, store_rows), cost=1.1, rank=1,
            sends=send_parts(f"r{k}", by_rows, k * run, run))
        scatter_sums(f"r{k}", by_rows, k * run, run, [f"p1{k}"], first_finish(k))
        add(f"i{k}", after=[f"r{k}4", "xiend"], work=pool_in_rows(k), cost=1.5, rank=1, sends=[remote(
            f"halo{k}", "next", lambda k=k: pool_in.at[k, pl.ds(run - HALO, HALO)], lambda k=k: halo.at[k + 1],
            (HALO, blocks * lane),
        )])

        def run_view(block, part, start=start):
            half = run // 2
            begin, extent = ((0, half), (half, half), (0, run))[part]
            return middle.at[pl.ds(pl.multiple_of(start + block * run + begin, half), extent)]

        add(f"m{k}", waits=[f"halo{k}"], after=[f"i{k}", "xoend"] + before, work=mixer_rows(k), cost=1.8, rank=1,
            sends=send_own(f"a{k}", run_view, run * model))
        seen = gather_blocks(f"a{k}", run_view, run * model)
        add(f"n2{k}", waits=seen["waits"], after=seen["after"] + [f"h1{k}"], cost=0.8, rank=2,
            work=functools.partial(
                normalize_rows, lambda b, place: middle[place, b * width:(b + 1) * width], second_gain, start))
        add(f"h2{k}", after=[f"n2{k}", f"p1{k}"] + ends("g2", "u2"), work=hidden_rows(1, start), cost=2.0, rank=2)

        def store_cols(n, value, rows=rows):
            for b in range(2):
                cols_part[n, b, rows] = value[:, b * width:(b + 1) * width]

        add(f"p2{k}", after=[f"h2{k}"] + ends("d2"), work=down_rows(1, start, store_cols), cost=1.1, rank=1,
            sends=send_parts(f"q{k}", by_cols, start, length))

        def last_finish(total, rows=rows):
            def work():
                cols = pl.ds(pl.multiple_of(tp * width, width), width)
                value = middle[rows, cols].astype(F32) + 0.5 * total(slice(None))
                out[rows, :] = value.astype(BF16)
            return work, [], 0.3

        scatter_sums(f"q{k}", by_cols, start, length, [f"p2{k}"], last_finish)
    return tasks, devices, counts


def layer_kernel(ring, *refs):
    fs, tp = lax.axis_index("fs"), lax.axis_index("tp")
    tasks, devices, counts = build(ring, fs, tp, refs)
    send_sem, recv_sem, local_sem = refs[-3:]
    assert counts["r"] == send_sem.shape[0] and counts["l"] == local_sem.shape[0], counts
    barrier = pltpu.get_barrier_semaphore()
    for device in devices.values():
        pl.semaphore_signal(barrier, inc=1, device_id=device, device_id_type=MESH)
    pl.semaphore_wait(barrier, len(devices))
    events, sent, waited = {}, [], set()
    for _, task in ordered(tasks):
        for event in task.waits:
            link, copy = events[event]
            copy.wait() if link == "l" else copy.wait_recv()
            waited.add(event)
        if task.work is not None:
            task.work()
        for event, link, _, make in task.sends:
            copy = make()
            copy.start()
            events[event] = (link, copy)
            if link != "l":
                sent.append(copy)
    assert waited == set(events)
    for copy in sent:
        copy.wait_send()


def scratch_of(ring, rows, width, units):
    blocks, run, lane = 2 * ring, rows // CHUNKS // (2 * ring), 128
    model, runs = blocks * width, rows // (2 * ring)
    remote_copies, local_copies = 7 * 16 + 8 + 16 + CHUNKS * 19, 9
    return [
        pltpu.VMEM((2, ring, ring, lane, units), BF16),
        pltpu.VMEM((2, ring, ring, lane, units), BF16),
        pltpu.VMEM((2, ring, ring, units, lane), BF16),
        pltpu.VMEM((blocks, ring, ring, 2 * lane, lane), BF16),
        pltpu.VMEM((blocks, rows, width), BF16),
        pltpu.VMEM((rows, model), BF16),
        pltpu.VMEM((rows, units), BF16),
        pltpu.VMEM((rows, model), BF16),
        pltpu.VMEM((run, model), BF16),
        pltpu.VMEM((runs, model), BF16),
        pltpu.VMEM((CHUNKS, run, blocks * lane), BF16),
        pltpu.VMEM((CHUNKS + 1, HALO, blocks * lane), BF16),
        pltpu.VMEM((run, blocks * lane), BF16),
        pltpu.VMEM((ring, 2, runs, model), BF16),
        pltpu.VMEM((ring, runs, model), BF16),
        pltpu.VMEM((2, runs // 2, model), BF16),
        pltpu.VMEM((2, runs, model), BF16),
        pltpu.VMEM((ring, 2, rows, width), BF16),
        pltpu.VMEM((ring, rows, width), BF16),
        pltpu.VMEM((2, rows // 2, width), BF16),
        pltpu.VMEM((2, rows, width), BF16),
        pltpu.SemaphoreType.DMA((remote_copies,)),
        pltpu.SemaphoreType.DMA((remote_copies,)),
        pltpu.SemaphoreType.DMA((local_copies,)),
    ]


def per_device(
    tokens, first_gain, first_gate, first_up, first_down, mix_gain, mix_input, pool_weight, pool_scale, mix_output,
    second_gain, second_gate, second_up, second_down, *, ring,
):
    rows, width = tokens.shape
    anywhere = pl.BlockSpec(memory_space=pl.ANY)
    inside = pl.BlockSpec(memory_space=pltpu.VMEM)
    return pl.pallas_call(
        functools.partial(layer_kernel, ring),
        out_shape=jax.ShapeDtypeStruct((rows, width), BF16),
        in_specs=[
            anywhere, inside, anywhere, anywhere, anywhere, inside, anywhere, inside, inside, anywhere,
            inside, anywhere, anywhere, anywhere,
        ],
        out_specs=inside,
        scratch_shapes=scratch_of(ring, rows, width, first_gate.shape[1]),
        compiler_params=pltpu.CompilerParams(collective_id=0, has_side_effects=True, vmem_limit_bytes=VMEM_LIMIT),
    )(
        tokens, first_gain.reshape(1, -1), first_gate, first_up, first_down, mix_gain.reshape(1, -1), mix_input,
        pool_weight, pool_scale.reshape(-1, 128), mix_output, second_gain.reshape(1, -1), second_gate, second_up,
        second_down,
    )


def solution(mesh):
    weight, turned = P("fs", "tp"), P("tp", "fs")
    return jax.shard_map(
        functools.partial(per_device, ring=mesh.shape["tp"] // 2),
        mesh=mesh,
        in_specs=(
            P("fs", "tp"), P(), weight, weight, turned, P(), weight, P(), P(), turned, P(), weight, weight, turned,
        ),
        out_specs=P("fs", "tp"),
        check_vma=False,
    )
```

time: 182 us -> 175 us (0.962)
  Pallas kernels: 179 us -> 172 us
    pallas_call x1, Pallas kernels: 179 us -> 172 us  [per_device(): pl.pallas_call(functools.partial(layer_kernel, ring), out_shape=jax.Shape...]
where the time goes in v2:
time: 175 us; the launch traced here: 174 us
  Pallas kernels  172 us (98%)
  local copies, waits for them, and re-layouts  1.87 us (1%)
    pallas_call x1, Pallas kernels, per_device(): pl.pallas_call(functools.partial(layer_kernel, ring), out_shape=jax.Shape...  172 us

profile of v2, /device:TPU:1, one launch (start us, length us, event | category | flops | bytes accessed | tf_op | source)
XLA Modules:
  0.0 174.4 jit_solution(86966826788295921)
XLA Ops:
  0.0 172.5 %shard_map.136 = bf16[1024,256]{1,0:T(8,128)(2,1)} custom-call(bf16[1024,256]{1,0:T(8,128)(2,1)} %refs_0_.1, f32[1,2048]{1,0:T(1,128)} %bitcast.4, bf16[128,768]{1,0:T(8,128)(2,1)} %refs_2_.1, bf16[128,768]{1,0:T(8,128)(2,1)} %refs_3_.1, bf16[768,128]{1,0:T(8,128)(2,1)} %refs_4_.1, f32[1,2048]{1,0:T(1,128)} %bitcast.5, bf16[128,128]{1,0:T(8,128)(2,1)} %refs_6_.1, ...), custom_call_target="tpu_custom_call" | custom-call | tf_op jit(solution)/shard_map/pallas_call | solution.py:506
  172.5 1.9 %copy.16 = bf16[1024,256]{1,0:T(8,128)(2,1)} copy(bf16[1024,256]{1,0:T(8,128)(2,1)} %shard_map.136) | data formatting | bytes 1048576
